TPU v7x, 512 devices: a 4x2x32 block of a 4x8x32 slice. The times are simulated.
512 devices in a mesh: grp: 2 (over y), sp: 64 (over z, core), tp: 4 (over x).
Axes of the slice: x: 4, y: 2, z: 32, core: 2. Of those that a mesh axis runs over, the one named last changes fastest.
The devices are a block of a 4x8x32 slice.
Arguments:
- query_latent: bfloat16 [16384, 768], P(('grp', 'sp')), parts along dimension 0, may hold values from -6 to 6
- key_latent: bfloat16 [16384, 256], P(('grp', 'sp', 'tp')), parts along dimension 0, may hold values from -20 to 20
- rotary_key: bfloat16 [16384, 64], P(('grp', 'sp', 'tp')), parts along dimension 0, may hold values from -1000 to 1000
- query_gain: float32 [768], replicated, may hold values from 0.1 to 1.9
- latent_gain: float32 [256], replicated, may hold values from 0.1 to 1.9
- query_up: bfloat16 [768, 3072], P(None, 'tp'), may hold values from -0.21875 to 0.21875
- key_up: bfloat16 [256, 2048], P(None, 'tp'), may hold values from -0.375 to 0.375
- value_up: bfloat16 [256, 2048], P(None, 'tp'), may hold values from -0.375 to 0.375
- out_gain: float32 [2048], P('tp'), may hold values from 0.1 to 1.9
- out_weight: bfloat16 [2048, 4096], P('sp', 'tp'), may hold values from -0.125 to 0.125
Outputs:
- mixed: bfloat16 [16384, 4096], P(('grp', 'sp'), 'tp'), parts along dimension 0
There are 2 independent parts, one for each index of `grp`. A program takes and returns all parts, laid end to end along the dimension named above; an argument that names none is the same for every part. Nothing has to cross between parts.
All inputs are finite; a program needn't handle non-finite values.
Results may differ from a plain program's by a relative error of at most 0.02.
The roundings to bfloat16 on the way count: a program that leaves them out, or rounds other values in their place, can miss the bound.
Values may be sent and summed in bfloat16 or wider, within the bound.
No kernel may reach another device: no remote copies, remote signals or barrier semaphores. Data moves between devices by JAX's collectives and lax.ppermute only.
A program may use at most 128 MiB of HBM per device.

v0:
```python
import jax
import jax.numpy as jnp
from jax import lax
from jax.sharding import PartitionSpec as P

HEADS = 16
NOPE_DIM = 128
ROPE_DIM = 64
VALUE_DIM = 128
KVRANK = 256
norm_eps = 1e-06
rope_theta = 10000.0


def side_by_side(arrays, axis, dim, along):
    widths = [a.shape[along] for a in arrays]
    both = jnp.concatenate(arrays, axis=along)
    filled = lax.all_gather(both, axis, axis=dim, tiled=True)
    return tuple(jnp.split(filled, [sum(widths[:k]) for k in range(1, len(widths))], axis=along))


def rms_scaled(inputs, gain_vec):
    widened = inputs.astype(jnp.float32)
    return (
        widened
        * lax.rsqrt(jnp.mean(widened * widened, axis=-1, keepdims=True) + norm_eps)
        * gain_vec
    )


def rotate_half(inputs, positions):
    half_width = inputs.shape[-1] // 2
    inverse = rope_theta ** (-jnp.arange(half_width, dtype=jnp.float32) / half_width)
    angles = positions[:, None] * inverse[None, :]
    if inputs.ndim == 3:
        angles = angles[:, None, :]
    cosine = jnp.cos(angles)
    sine = jnp.sin(angles)
    widened = inputs.astype(jnp.float32)
    first = widened[..., :half_width]
    second = widened[..., half_width:]
    return jnp.concatenate(
        [first * cosine - second * sine, second * cosine + first * sine], axis=-1
    )


def on_device(
    query_latent,
    key_latent,
    rotary_key,
    query_gain,
    latent_gain,
    query_up,
    key_up,
    value_up,
    out_gain,
    out_weight,
):
    block_rows = query_latent.shape[0]
    row_count = key_latent.shape[0]
    head_local = key_up.shape[1] // NOPE_DIM
    block_start = lax.axis_index("sp") * block_rows
    own_start = block_start + lax.axis_index("tp") * row_count
    score_scale = (NOPE_DIM + ROPE_DIM) ** (-0.5)
    normed = rms_scaled(query_latent, query_gain).astype(jnp.bfloat16)
    query_full = jnp.dot(normed, query_up, preferred_element_type=jnp.float32).astype(jnp.bfloat16)
    query_full = query_full.reshape(block_rows, head_local, NOPE_DIM + ROPE_DIM)
    query_positions = (block_start + jnp.arange(block_rows, dtype=jnp.int32)).astype(jnp.float32)
    query_plain = query_full[..., :NOPE_DIM]
    query_turned = rotate_half(query_full[..., NOPE_DIM:], query_positions).astype(jnp.bfloat16)
    latent_normed = rms_scaled(key_latent, latent_gain).astype(jnp.bfloat16)
    own_positions = (own_start + jnp.arange(row_count, dtype=jnp.int32)).astype(jnp.float32)
    key_turned = rotate_half(rotary_key, own_positions).astype(jnp.bfloat16)
    block_latents, block_keys = side_by_side((latent_normed, key_turned), "tp", 0, 1)
    running_max = jnp.full((block_rows, head_local), -1e30, jnp.float32)
    running_sum = jnp.zeros((block_rows, head_local), jnp.float32)
    weighted = jnp.zeros((block_rows, head_local, KVRANK), jnp.float32)
    latents, turned_keys = side_by_side((block_latents, block_keys), "sp", 0, 1)
    portion_rows = latents.shape[0]
    step_rows = min(portion_rows, 2048)
    for begin in range(0, portion_rows, step_rows):
        latent_part = latents[begin : begin + step_rows]
        turned_part = turned_keys[begin : begin + step_rows]
        key_plain = jnp.dot(latent_part, key_up, preferred_element_type=jnp.float32).astype(
            jnp.bfloat16
        )
        key_plain = key_plain.reshape(latent_part.shape[0], head_local, NOPE_DIM)
        scores = jnp.einsum(
            "qhd,khd->qhk", query_plain, key_plain, preferred_element_type=jnp.float32
        )
        scores = scores + jnp.einsum(
            "qhd,kd->qhk", query_turned, turned_part, preferred_element_type=jnp.float32
        )
        scores = scores * score_scale
        new_max = jnp.maximum(running_max, jnp.max(scores, axis=-1))
        rescale = jnp.exp(running_max - new_max)
        expo = jnp.exp(scores - new_max[..., None])
        running_sum = running_sum * rescale + jnp.sum(expo, axis=-1)
        weighted = weighted * rescale[..., None] + jnp.einsum(
            "qhk,kc->qhc",
            expo.astype(jnp.bfloat16),
            latent_part,
            preferred_element_type=jnp.float32,
        )
        running_max = new_max
    final_state = (running_max, running_sum, weighted)
    running_max, running_sum, weighted = final_state
    latent_mix = (weighted / running_sum[..., None]).astype(jnp.bfloat16)
    value_heads = value_up.reshape(KVRANK, head_local, VALUE_DIM)
    head_out = jnp.einsum(
        "qhc,chd->qhd", latent_mix, value_heads, preferred_element_type=jnp.float32
    ).astype(jnp.bfloat16)
    head_out = head_out.reshape(block_rows, head_local * VALUE_DIM)
    widened = head_out.astype(jnp.float32)
    square_part = jnp.sum(widened * widened, axis=1)
    gained = (widened * out_gain).astype(jnp.bfloat16)
    all_gained, square_parts = (
        lax.all_gather(gained, "tp", axis=1, tiled=True),
        lax.all_gather(square_part[:, None].astype(jnp.bfloat16), "tp", axis=1, tiled=True).astype(
            jnp.float32
        ),
    )
    all_squares = jnp.sum(square_parts, axis=1)
    own_sums = jnp.dot(
        all_gained,
        lax.all_gather(out_weight, "sp", axis=0, tiled=True),
        preferred_element_type=jnp.float32,
    )
    mean_square = all_squares / (HEADS * VALUE_DIM)
    return (own_sums * lax.rsqrt(mean_square + norm_eps)[:, None]).astype(jnp.bfloat16)


def solution(mesh):
    in_specs = (
        P(("grp", "sp"), None),
        P(("grp", "sp", "tp"), None),
        P(("grp", "sp", "tp"), None),
        P(),
        P(),
        P(None, "tp"),
        P(None, "tp"),
        P(None, "tp"),
        P("tp"),
        P("sp", "tp"),
    )
    out_specs = P(("grp", "sp"), "tp")
    return jax.shard_map(
        on_device, mesh=mesh, in_specs=in_specs, out_specs=out_specs, check_vma=False
    )
```

profile of v0, /device:TPU:33, one launch (start us, length us, event | category | flops | bytes accessed | tf_op | source)
XLA Modules:
  0.0 333.3 jit_solution(3699053288763499415)
XLA Ops:
  6.6 0.8 convert_element_type.106
  7.4 0.8 fusion.91
  8.2 0.8 fusion.93
  9.3 10.5 %all_gather.15 = bf16[128,320]{1,0:T(8,128)(2,1)S(1)} all-gather(bf16[32,320]{1,0:T(8,128)(2,1)S(1)} %pad_maximum_fusion.1), channel_id=1, replica_groups=mesh['grp'=2,'sp'=64,'tp'=4] {'tp'}, dimensions={0}, use_global_device_ids=true | all-gather | bytes 102400 | tf_op jit(solution)/shard_map/all_gather | solution.py:18
  19.7 0.7 copy.37
  20.6 0.7 all-gather.6.cloned.1.call-update
  21.4 1.0 fusion.75
  22.4 1.3 convolution_convert_fusion.4
  24.1 1.1 copy.77
  25.2 167.6 %all-gather.4.cloned.1.call-done = bf16[8192,320]{0,1:T(8,128)(2,1)} async-done(((bf16[128,320]{0,1:T(8,128)(2,1)}), bf16[8192,320]{0,1:T(8,128)(2,1)}) %all-gather.4.cloned.1.call-update) | async-done | bytes 5242896 | tf_op jit(solution)/shard_map/all_gather | solution.py:18
  192.8 2.2 convolution_convert_fusion.3
  195.0 2.0 convolution_convert_fusion
  197.0 0.8 convolution_convert_fusion.1
  197.7 0.8 convolution_convert_fusion.2
  198.5 0.9 fusion.87
  199.4 0.9 fusion.89
  200.3 0.9 fusion.83
  201.2 0.9 fusion.85
  202.1 0.8 fusion.108
  202.8 0.8 fusion.105
  203.6 0.8 fusion.106
  204.4 0.8 fusion.107
  205.2 1.1 fusion.4
  206.3 1.1 fusion.8
  207.4 1.0 fusion.27
  208.4 0.8 fusion.33
  209.2 0.8 fusion.39
  210.0 3.5 %multiply_reduce_fusion = (bf16[128]{0:T(256)(128)(2,1)S(1)}, f32[4,128,128]{1,2,0:T(8,128)S(1)}) fusion(bf16[256,4,128]{0,2,1:T(8,128)(2,1)S(1)} %bitcast.87, f32[128,4,256]{2,0,1:T(8,128)S(1)} %fusion.39, f32[128,4,2048]{0,2,1:T(8,128)} %copy-done.1, f32[128,4]{0,1:T(4,128)S(1)} %get-tuple-element.9, bf16[8192,320]{0,1:T(8,128)(2,1)} %all-gather.4.cloned.1.call-done, ...), kind=kOutput, calls=%fused_computation.70 | convolution fusion | flops 573177728 | bytes 6295808 | tf_op jit(solution)/shard_map/qhc,chd->qhd/dot_general | solution.py:110
  213.4 7.7 %all-gather = bf16[4,1,128]{2,1,0:T(2,128)(2,1)S(1)} all-gather(bf16[1,1,128]{2,1,0:T(2,128)(2,1)S(1)} %bitcast.88), channel_id=1, replica_groups=mesh['grp'=2,'sp'=64,'tp'=4] {'tp'}, dimensions={0}, use_global_device_ids=true | all-gather | bytes 1280 | tf_op jit(solution)/shard_map/all_gather | solution.py:119
  221.3 10.5 %all_gather.17 = bf16[128,2048]{0,1:T(8,128)(2,1)S(1)} all-gather(bf16[128,512]{0,1:T(8,128)(2,1)S(1)} %fusion.78), channel_id=1, replica_groups=mesh['grp'=2,'sp'=64,'tp'=4] {'tp'}, dimensions={1}, use_global_device_ids=true | all-gather | bytes 655360 | tf_op jit(solution)/shard_map/all_gather | solution.py:118
  231.8 91.0 %all-gather.6.cloned.1.call-done = bf16[2048,1024]{1,0:T(8,128)(2,1)} async-done(((bf16[32,1024]{1,0:T(8,128)(2,1)}), bf16[2048,1024]{1,0:T(8,128)(2,1)}) %all-gather.6.cloned.1.call-update) | async-done | bytes 4194320 | tf_op jit(solution)/shard_map/all_gather | solution.py:126
  322.8 3.6 %fusion.45 = bf16[128,1024]{1,0:T(8,128)(2,1)} fusion(bf16[128,2048]{0,1:T(8,128)(2,1)S(1)} %all_gather.17, bf16[2048,1024]{1,0:T(8,128)(2,1)} %all-gather.6.cloned.1.call-done, f32[128]{0:T(128)S(1)} %add_rsqrt_fusion), kind=kOutput, calls=%fused_computation.40 | convolution fusion | flops 537133056 | bytes 4981248 | tf_op jit(solution)/shard_map/dot_general | solution.py:124
  (29 shorter events, 0.9 us)
Async XLA Ops:
  6.5 15.9 %copy-start = (bf16[768,768]{1,0:T(8,128)(2,1)S(1)}, bf16[768,768]{1,0:T(8,128)(2,1)}, u32[]{:S(2)}) copy-start(bf16[768,768]{1,0:T(8,128)(2,1)} %param.15) | copy-start | bytes 3538948
  6.6 188.4 %copy-start.3 = (bf16[256,512]{1,0:T(8,128)(2,1)S(1)}, bf16[256,512]{1,0:T(8,128)(2,1)}, u32[]{:S(2)}) copy-start(bf16[256,512]{1,0:T(8,128)(2,1)} %param.16) | copy-start | bytes 786436
  6.6 186.2 %all-gather.4.cloned.1.call-start = ((), (), s32[]{:S(2)}) async-start(), calls=%async_computation | async-start | bytes 5324800 | tf_op jit(solution)/shard_map/all_gather | solution.py:18
  20.5 302.2 %all-gather.6.cloned.1.call-start = ((), (), s32[]{:S(2)}) async-start(), calls=%async_computation.1 | async-start | bytes 4259840 | tf_op jit(solution)/shard_map/all_gather | solution.py:126
  192.8 4.2 %copy-start.2 = (bf16[8192,320]{0,1:T(8,128)(2,1)S(1)}, bf16[8192,320]{0,1:T(8,128)(2,1)}, u32[]{:S(2)}) copy-start(bf16[8192,320]{0,1:T(8,128)(2,1)} %all-gather.4.cloned.1.call-done) | copy-start | bytes 15728644
  203.6 2.7 copy-start.1
  209.9 11.2 %copy-start.4 = (f32[512]{0:T(512)S(1)}, f32[512]{0:T(512)}, u32[]{:S(2)}) copy-start(f32[512]{0:T(512)} %param.18) | copy-start | bytes 6148
Sparse Core Ops, SparseCore 0:
  20.7 172.0 all-gather.3
  194.9 127.8 all-gather.5
where the time goes:
time: 334 us; the launch traced here: 333 us
  waiting for transfers between devices  259 us (78%)
  blocking collectives  28.7 us (9%)
  matrix products  23.1 us (7%)
  between operations  13.6 us (4%)
  other arithmetic  6.34 us (2%)
    all_gather x1, waiting for transfers between devices, side_by_side(): filled = lax.all_gather(both, axis, axis=dim, tiled=True)  168 us
    all_gather x1, waiting for transfers between devices, on_device(): lax.all_gather(out_weight, 'sp', axis=0, tiled=True)  91 us
    all_gather x1, blocking collectives, on_device(): lax.all_gather(gained, 'tp', axis=1, tiled=True)  10.5 us
    all_gather x1, blocking collectives, side_by_side(): filled = lax.all_gather(both, axis, axis=dim, tiled=True)  10.5 us
    all_gather x1, blocking collectives, on_device(): lax.all_gather(square_part[:, None].astype(jnp.bfloat16), 'tp', axis=1, t...  7.7 us
  transfers between devices with their start and end apart: 2, of which 2 were waited for; matrix products, arithmetic and copies ran while one was open for 7% of the time, Pallas kernels for 0%

commit v1 on v0

--- a/solution.py
+++ b/solution.py
@@ -10,6 +10,13 @@
 KVRANK = 256
 norm_eps = 1e-06
 rope_theta = 10000.0
+
+
+def all_by_exchange(x, axis, dim):
+    devices = lax.axis_size(axis)
+    parts = jnp.stack([x for _ in range(devices)])
+    parts = lax.all_to_all(parts, axis, split_axis=0, concat_axis=0)
+    return jnp.concatenate(parts, axis=dim)
 
 
 def side_by_side(arrays, axis, dim, along):
@@ -122,9 +129,7 @@
     )
     all_squares = jnp.sum(square_parts, axis=1)
     own_sums = jnp.dot(
-        all_gained,
-        lax.all_gather(out_weight, "sp", axis=0, tiled=True),
-        preferred_element_type=jnp.float32,
+        all_gained, all_by_exchange(out_weight, "sp", 0), preferred_element_type=jnp.float32
     )
     mean_square = all_squares / (HEADS * VALUE_DIM)
     return (own_sums * lax.rsqrt(mean_square + norm_eps)[:, None]).astype(jnp.bfloat16)

time: 334 us -> 521 us (1.56)
  waiting for transfers between devices: 259 us -> 393 us
  starting transfers between devices: 0.07 us -> 47.7 us
    all_gather x1, waiting for transfers between devices: 168 us -> 393 us  [side_by_side(): filled = lax.all_gather(both, axis, axis=dim, tiled=True)]
    all_gather x1 -> x0, waiting for transfers between devices: 91 us -> none  [on_device(): lax.all_gather(out_weight, 'sp', axis=0, tiled=True)]
    all_to_all x0 -> x1, starting transfers between devices: none -> 47.6 us  [all_by_exchange(): parts = lax.all_to_all(parts, axis, split_axis=0, concat_axis=0)]
  transfers between devices with their start and end apart: 2 -> 2, of which waited for: 2 -> 1; matrix products, arithmetic and copies ran while one was open for 7% -> 4% of each run, Pallas kernels for 0% -> 0%
where the time goes in v1:
time: 521 us; the launch traced here: 516 us
  waiting for transfers between devices  393 us (75%)
  starting transfers between devices  47.7 us (9%)
  blocking collectives  32.2 us (6%)
  matrix products  22 us (4%)
  between operations  13.7 us (3%)
    all_gather x1, waiting for transfers between devices, side_by_side(): filled = lax.all_gather(both, axis, axis=dim, tiled=True)  393 us
    all_to_all x1, starting transfers between devices, all_by_exchange(): parts = lax.all_to_all(parts, axis, split_axis=0, concat_axis=0)  47.6 us
    all_gather x1, blocking collectives, side_by_side(): filled = lax.all_gather(both, axis, axis=dim, tiled=True)  11.2 us
    all_gather x1, blocking collectives, on_device(): lax.all_gather(square_part[:, None].astype(jnp.bfloat16), 'tp', axis=1, t...  10.8 us
  transfers between devices with their start and end apart: 2, of which 1 were waited for; matrix products, arithmetic and copies ran while one was open for 4% of the time, Pallas kernels for 0%

profile of v1, /device:TPU:33, one launch (start us, length us, event | category | flops | bytes accessed | tf_op | source)
XLA Modules:
  0.0 516.3 jit_solution(12219983268907171532)
XLA Ops:
  6.6 3.5 stack.2
  10.1 47.6 %all-to-all-start = ((bf16[64,32,1024]{2,1,0:T(8,128)(2,1)}), bf16[64,32,1024]{2,1,0:T(8,128)(2,1)}, u32[]{:S(2)}, u32[]{:S(2)}) async-start(bf16[64,32,1024]{2,1,0:T(8,128)(2,1)} %stack.2), calls=%async_computation | async-start | bytes 8388608 | tf_op jit(solution)/shard_map/all_to_all | solution.py:18
  58.0 0.1 fusion.99
  58.3 11.2 %all_gather.12 = bf16[128,320]{1,0:T(8,128)(2,1)S(1)} all-gather(bf16[32,320]{1,0:T(8,128)(2,1)S(1)} %pad_maximum_fusion.1), channel_id=1, replica_groups=mesh['grp'=2,'sp'=64,'tp'=4] {'tp'}, dimensions={0}, use_global_device_ids=true | all-gather | bytes 102400 | tf_op jit(solution)/shard_map/all_gather | solution.py:25
  69.5 0.7 copy.37
  70.5 0.4 convolution_convert_fusion.4
  70.8 0.2 copy.38
  71.0 0.1 copy.77
  71.2 0.1 multiply_cosine_fusion
  71.3 392.6 %all-gather.3.cloned.1.call-done = bf16[8192,320]{0,1:T(8,128)(2,1)} async-done(((bf16[128,320]{0,1:T(8,128)(2,1)}), bf16[8192,320]{0,1:T(8,128)(2,1)}) %all-gather.3.cloned.1.call-update) | async-done | bytes 5242896 | tf_op jit(solution)/shard_map/all_gather | solution.py:25
  463.9 2.1 convolution_convert_fusion.3
  466.1 2.0 convolution_convert_fusion
  468.0 0.8 convolution_convert_fusion.1
  468.8 0.8 convolution_convert_fusion.2
  469.6 0.9 fusion.87
  470.5 0.9 fusion.89
  471.4 0.9 fusion.83
  472.3 0.9 fusion.85
  473.2 0.8 fusion.108
  473.9 0.8 fusion.105
  474.7 0.8 fusion.106
  475.5 0.8 fusion.107
  476.3 1.1 fusion.4
  477.4 1.3 fusion.8
  478.8 0.8 fusion.27
  479.5 0.8 fusion.33
  480.3 0.8 fusion.39
  481.1 3.5 multiply_reduce_fusion
  484.5 10.8 %all-gather = bf16[4,1,128]{2,1,0:T(2,128)(2,1)S(1)} all-gather(bf16[1,1,128]{2,1,0:T(2,128)(2,1)S(1)} %bitcast.89), channel_id=1, replica_groups=mesh['grp'=2,'sp'=64,'tp'=4] {'tp'}, dimensions={0}, use_global_device_ids=true | all-gather | bytes 1280 | tf_op jit(solution)/shard_map/all_gather | solution.py:126
  495.3 0.1 fusion.78
  495.5 10.3 %all_gather.14 = bf16[128,2048]{0,1:T(8,128)(2,1)S(1)} all-gather(bf16[128,512]{0,1:T(8,128)(2,1)S(1)} %fusion.78), channel_id=1, replica_groups=mesh['grp'=2,'sp'=64,'tp'=4] {'tp'}, dimensions={1}, use_global_device_ids=true | all-gather | bytes 655360 | tf_op jit(solution)/shard_map/all_gather | solution.py:125
  505.8 3.6 fusion.45
  (41 shorter events, 0.7 us)
Async XLA Ops:
  6.5 63.9 %copy-start = (bf16[768,768]{1,0:T(8,128)(2,1)S(1)}, bf16[768,768]{1,0:T(8,128)(2,1)}, u32[]{:S(2)}) copy-start(bf16[768,768]{1,0:T(8,128)(2,1)} %param.15) | copy-start | bytes 3538948
  10.1 47.7 %copy-start.7 = (bf16[32,64]{1,0:T(8,128)(2,1)S(1)}, bf16[32,64]{1,0:T(8,128)(2,1)}, u32[]{:S(2)}) copy-start(bf16[32,64]{1,0:T(8,128)(2,1)} %param.12) | copy-start | bytes 12292
  10.1 47.8 %copy-start.6 = (bf16[32,256]{1,0:T(8,128)(2,1)S(1)}, bf16[32,256]{1,0:T(8,128)(2,1)}, u32[]{:S(2)}) copy-start(bf16[32,256]{1,0:T(8,128)(2,1)} %param.11) | copy-start | bytes 49156
  10.1 48.1 %copy-start.10 = (f32[256]{0:T(256)S(1)}, f32[256]{0:T(256)}, u32[]{:S(2)}) copy-start(f32[256]{0:T(256)} %param.14) | copy-start | bytes 3076
  10.1 60.2 %copy-start.4 = (bf16[128,768]{1,0:T(8,128)(2,1)S(1)}, bf16[128,768]{1,0:T(8,128)(2,1)}, u32[]{:S(2)}) copy-start(bf16[128,768]{1,0:T(8,128)(2,1)} %param.10) | copy-start | bytes 589828
  10.1 60.4 %copy-start.8 = (f32[768]{0:T(1024)S(1)}, f32[768]{0:T(1024)}, u32[]{:S(2)}) copy-start(f32[768]{0:T(1024)} %param.13) | copy-start | bytes 9220
  10.1 60.9 %copy-start.5 = (bf16[256,512]{1,0:T(8,128)(2,1)S(1)}, bf16[256,512]{1,0:T(8,128)(2,1)}, u32[]{:S(2)}) copy-start(bf16[256,512]{1,0:T(8,128)(2,1)} %param.17) | copy-start | bytes 786436
  10.1 453.8 %copy-start.3 = (bf16[256,512]{1,0:T(8,128)(2,1)S(1)}, bf16[256,512]{1,0:T(8,128)(2,1)}, u32[]{:S(2)}) copy-start(bf16[256,512]{1,0:T(8,128)(2,1)} %param.16) | copy-start | bytes 786436
  10.1 495.6 %all-to-all-start = ((bf16[64,32,1024]{2,1,0:T(8,128)(2,1)}), bf16[64,32,1024]{2,1,0:T(8,128)(2,1)}, u32[]{:S(2)}, u32[]{:S(2)}) async-start(bf16[64,32,1024]{2,1,0:T(8,128)(2,1)} %stack.2), calls=%async_computation | async-start | bytes 8388608 | tf_op jit(solution)/shard_map/all_to_all | solution.py:18
  57.7 406.2 %all-gather.3.cloned.1.call-start = ((), (), s32[]{:S(2)}) async-start(), calls=%async_computation.1 | async-start | bytes 5324800 | tf_op jit(solution)/shard_map/all_gather | solution.py:25
  463.9 4.1 copy-start.2
  474.7 2.7 copy-start.1
  481.1 14.3 %copy-start.9 = (f32[512]{0:T(512)S(1)}, f32[512]{0:T(512)}, u32[]{:S(2)}) copy-start(f32[512]{0:T(512)} %param.18) | copy-start | bytes 6148
Sparse Core Ops, SparseCore 0:
  70.4 393.4 all-gather.2
